TPU v7x, 32 devices: a whole 2x2x4 slice. The times are simulated.
32 devices in a mesh: sp: 8 (over z, y), tp: 4 (over x, core).
Axes of the slice: x: 2, y: 2, z: 4, core: 2. Of those that a mesh axis runs over, the one named last changes fastest.
Arguments:
- resid_in: bfloat16 [2048, 2048], P('sp'), may hold values from -6 to 6
- query_latent: bfloat16 [2048, 768], P('sp'), may hold values from -6 to 6
- kv_latent: bfloat16 [2048, 512], P('sp'), may hold values from -6 to 6
- rotary_key: bfloat16 [2048, 64], P('sp'), may hold values from -200 to 200
- query_gain: float32 [768], replicated, may hold values from 0.1 to 1.9
- kv_gain: float32 [512], replicated, may hold values from 0.1 to 1.9
- w_query_plain: bfloat16 [768, 2048], P(None, 'tp'), may hold values from -0.875 to 0.875
- w_query_rotary: bfloat16 [768, 1024], P(None, 'tp'), may hold values from -0.875 to 0.875
- w_key_plain: bfloat16 [512, 2048], P(None, 'tp'), may hold values from -0.25 to 0.25
- w_value: bfloat16 [512, 2048], P(None, 'tp'), may hold values from -0.25 to 0.25
- w_output: bfloat16 [2048, 2048], P('tp'), may hold values from -0.125 to 0.125
- ffn_gain: float32 [2048], replicated, may hold values from 0.1 to 1.9
- w_gate: bfloat16 [2048, 5632], P('sp', 'tp'), may hold values from -0.125 to 0.125
- w_up: bfloat16 [2048, 5632], P('sp', 'tp'), may hold values from -0.125 to 0.125
- w_down: bfloat16 [5632, 2048], P('tp', 'sp'), may hold values from -0.078125 to 0.078125
Outputs:
- resid_out: bfloat16 [2048, 2048], P(('sp', 'tp'))
All inputs are finite; a program needn't handle non-finite values.
Results may differ from a plain program's by a relative error of at most 0.014.
The roundings to bfloat16 on the way count: a program that leaves them out, or rounds other values in their place, can miss the bound.
Values may be sent and summed in bfloat16 or wider, within the bound.
A program may use at most 192 MiB of HBM per device.

v0:
```python
import functools

import jax
import jax.numpy as jnp
from jax import lax
from jax.experimental import pallas as pl
from jax.experimental.pallas import tpu as pltpu
from jax.sharding import PartitionSpec as P

NOPE = 128
ROPE = 64
VDIM = 128
MESH = pl.DeviceIdType.MESH


def normed(values, gain):
    wide = values.astype(jnp.float32)
    return wide * lax.rsqrt(jnp.mean(wide * wide, axis=-1, keepdims=True) + 1e-06) * gain


def rotate(values, cosine, sine):
    half = values.shape[-1] // 2
    first = values[..., :half]
    second = values[..., half:]
    return jnp.concatenate(
        [first * cosine - second * sine, second * cosine + first * sine], axis=-1
    )


class Plan:
    def __init__(self, sp, tp):
        self.sp, self.tp = sp, tp
        self.z = 4 if sp % 4 == 0 else 1
        self.r = sp // self.z
        self.c = 2 if tp % 2 == 0 else 1
        self.x = tp // self.c

    def sizes(self):
        return {"z": self.z, "r": self.r, "x": self.x, "c": self.c}

    def here(self):
        s, t = lax.axis_index("sp"), lax.axis_index("tp")
        return {"z": s // self.r, "r": lax.rem(s, self.r), "x": t // self.c, "c": lax.rem(t, self.c)}

    def device(self, at):
        return {"sp": at["z"] * self.r + at["r"], "tp": at["x"] * self.c + at["c"]}

    def shifted(self, at, axis, by):
        size = self.sizes()[axis]
        return {**at, axis: lax.rem(at[axis] + (by % size), size)}


def front_body(
    plan,
    heads,
    part,
    kv_ref,
    qp_ref,
    qr_ref,
    wk_ref,
    wv_ref,
    wo_ref,
    resid_ref,
    gain_ref,
    gate_ref,
    up_ref,
    down_ref,
    o_ref,
    mid_ref,
    hn_ref,
    both_ref,
    downs_ref,
    packed,
    attn,
    out,
    terms,
    h_own,
    part_ref,
    got_c,
    sum_c,
    got_x,
    sum_x,
    got_z,
    kv_sa,
    kv_ra,
    kv_sb,
    kv_rb,
    kv_sc,
    kv_rc,
    hn_sa,
    hn_ra,
    hn_sb,
    hn_rb,
    hn_sc,
    hn_rc,
    w_sa,
    w_ra,
    w_sb,
    w_rb,
    t_s,
    t_r,
    c_s,
    c_r,
    x_s,
    x_r,
    z_s,
    z_r,
    local,
):
    here = plan.here()
    sizes = plan.sizes()
    nz, nr, tp = plan.z, plan.r, plan.tp
    latent = wk_ref.shape[0]
    depth, full = gate_ref.shape
    narrow = down_ref.shape[1]
    sp_here, tp_here = lax.axis_index("sp"), lax.axis_index("tp")

    barrier = pltpu.get_barrier_semaphore()
    peers = [plan.shifted(here, "z", k) for k in range(1, nz)]
    peers += [plan.shifted(here, "r", k) for k in range(1, nr)]
    peers = [plan.device(at) for at in peers]
    peers += [{"sp": sp_here, "tp": lax.rem(tp_here + k, tp)} for k in range(1, tp)]
    for peer in peers:
        pl.semaphore_signal(barrier, inc=1, device_id=peer, device_id_type=MESH)
    pl.semaphore_wait(barrier, len(peers))

    def send(src, dst, device, sem_s, sem_r):
        copy = pltpu.make_async_remote_copy(
            src_ref=src,
            dst_ref=dst,
            send_sem=sem_s,
            recv_sem=sem_r,
            device_id=device,
            device_id_type=MESH,
        )
        copy.start()
        return copy

    class Gather:
        def __init__(self, axes, x_ref, o_ref, sems, own):
            self.axes, self.x_ref, self.o_ref, self.sems = axes, x_ref, o_ref, sems
            self.copies = {}
            self.mine = pltpu.make_async_copy(x_ref, o_ref.at[self.slot(here)], own)

        def slot(self, at):
            index = 0
            for axis in self.axes:
                index = index * sizes[axis] + at[axis]
            return index

        def send(self, stage, block, by, key):
            mine = len(key) == 0 or not any(key)
            src = self.x_ref if mine else self.o_ref.at[self.slot(block)]
            sem_s, sem_r = self.sems[2 * stage], self.sems[2 * stage + 1]
            at = (key + (by,)) if stage else by
            self.copies[key + (by,)] = send(
                src,
                self.o_ref.at[self.slot(block)],
                plan.device(plan.shifted(here, self.axes[stage], by)),
                sem_s.at[at],
                sem_r.at[at],
            )

        def start(self):
            self.mine.start()
            for k in range(1, sizes[self.axes[0]]):
                self.send(0, here, k, ())

        def relay(self, k):
            block = plan.shifted(here, self.axes[0], -k)
            if k:
                self.copies[(k,)].wait_recv()
            for j in range(1, sizes[self.axes[1]]):
                self.send(1, block, j, (k,))
            for l in range(1, sizes[self.axes[2]]):
                self.send(2, block, l, (k, 0))

        def relay_on(self, k):
            for j in range(1, sizes[self.axes[1]]):
                self.copies[(k, j)].wait_recv()
                block = plan.shifted(here, self.axes[0], -k)
                block = plan.shifted(block, self.axes[1], -j)
                for l in range(1, sizes[self.axes[2]]):
                    self.send(2, block, l, (k, j))

        def landed(self, k):
            if k == 0:
                self.mine.wait()
            for key, copy in self.copies.items():
                if len(key) == 3 and key[0] == k:
                    copy.wait_recv()

        def finish(self):
            for copy in self.copies.values():
                copy.wait_send()

    def window(index):
        return pl.multiple_of(jnp.minimum(index * part, full - part), 128)

    def targets(sp):
        rows = pl.ds(pl.multiple_of(sp * depth, depth), depth)
        if len(downs_ref.shape) == 3:
            downs = downs_ref.at[sp]
        else:
            downs = downs_ref.at[:, pl.ds(pl.multiple_of(sp * narrow, 128), narrow)]
        return [
            both_ref.at[rows, pl.ds(0, part)],
            both_ref.at[rows, pl.ds(part, part)],
            downs,
        ]

    def sources(index):
        lanes = pl.ds(window(index), part)
        return [gate_ref.at[:, lanes], up_ref.at[:, lanes], down_ref.at[lanes, :]]

    kv = Gather(("z", "r", "c"), kv_ref, packed, (kv_sa, kv_ra, kv_sb, kv_rb, kv_sc, kv_rc), local.at[0])
    kv.start()
    over_z, over_r = {}, {}
    mine = []
    for w in range(3):
        src, dst = sources(here["z"])[w], targets(sp_here)[w]
        mine.append(pltpu.make_async_copy(src, dst, local.at[2 + w]))
        mine[-1].start()
        for k in range(1, nz):
            to = plan.shifted(here, "z", k)
            over_z[w, k] = send(
                sources(to["z"])[w], dst, plan.device(to), w_sa.at[w, k], w_ra.at[w, k]
            )
    for k in range(nz):
        kv.relay(k)
    for k in range(nz):
        kv.relay_on(k)

    def forward(w, k):
        block = plan.shifted(here, "z", -k)
        dst = targets(block["z"] * nr + here["r"])[w]
        src = dst if k else sources(here["z"])[w]
        if k:
            over_z[w, k].wait_recv()
        for j in range(1, nr):
            over_r[w, k, j] = send(
                src,
                dst,
                plan.device(plan.shifted(here, "r", j)),
                w_sb.at[w, k, j],
                w_rb.at[w, k, j],
            )

    for w in range(3):
        forward(w, 0)
    for k in range(nz):
        kv.landed(k)

    scale = (NOPE + ROPE) ** (-0.5)
    count = packed.shape[0] * packed.shape[1]

    def transposed(left, right):
        return lax.dot_general(
            left, right, (((1,), (1,)), ((), ())), preferred_element_type=jnp.float32
        )

    @pl.loop(0, heads)
    def _(h):
        lanes = pl.ds(pl.multiple_of(h * NOPE, NOPE), NOPE)
        lat = packed[:, :, :latent].reshape(count, latent)
        rot = packed[:, :, latent:].reshape(count, ROPE)
        keys = jnp.dot(lat, wk_ref[:, lanes], preferred_element_type=jnp.float32)
        vals = jnp.dot(lat, wv_ref[:, lanes], preferred_element_type=jnp.float32)
        keys, vals = keys.astype(jnp.bfloat16), vals.astype(jnp.bfloat16)
        score = (transposed(qp_ref[:, lanes], keys) + transposed(qr_ref[h], rot)) * scale
        weight = jnp.exp(score - jnp.max(score, axis=-1, keepdims=True))
        total = jnp.sum(weight, axis=-1, keepdims=True)
        mixed = jnp.dot(weight.astype(jnp.bfloat16), vals, preferred_element_type=jnp.float32)
        attn[:, lanes] = (mixed / total).astype(jnp.bfloat16)

    for k in range(1, nz):
        forward(0, k)
    share = out.shape[1]
    swaps = []
    for k in list(range(1, tp)) + [0]:
        to = lax.rem(tp_here + k, tp)
        rows = pl.ds(pl.multiple_of(to * share, share), share)
        out[to] = jnp.dot(
            attn[rows, :], wo_ref[...], preferred_element_type=jnp.float32
        ).astype(jnp.bfloat16)
        if k:
            swaps.append(
                send(out.at[to], terms.at[k], {"sp": sp_here, "tp": to}, t_s.at[k], t_r.at[k])
            )
    for k in range(1, nz):
        forward(1, k)
    mid = resid_ref[...].astype(jnp.float32) + out[tp_here].astype(jnp.float32)
    for k, copy in enumerate(swaps, 1):
        copy.wait_recv()
        mid += terms[k].astype(jnp.float32)
    mid_ref[...] = mid
    h_own[...] = (
        mid * lax.rsqrt(jnp.mean(mid * mid, axis=-1, keepdims=True) + 1e-06) * gain_ref[...]
    ).astype(jnp.bfloat16)
    hn = Gather(("z", "x", "c"), h_own, hn_ref, (hn_sa, hn_ra, hn_sb, hn_rb, hn_sc, hn_rc), local.at[1])
    hn.start()
    hn.relay(0)
    for k in range(1, nz):
        forward(2, k)
    for copy in over_r.values():
        copy.wait_recv()
    for copy in mine:
        copy.wait()

    nx, nc = plan.x, plan.c
    x, c = here["x"], here["c"]
    place = here["z"] * part
    lane = lax.broadcasted_iota(jnp.int32, (1, part), 1)
    fresh = lane >= place - jnp.minimum(place, full - part)
    wide = jnp.float32
    over_c, over_x, back = {}, {}, {}

    def feed(k):
        first = plan.shifted(here, "z", -k)["z"] * tp
        rows = hn_ref[pl.ds(first, tp)].reshape(tp * share, -1)
        inner = jnp.dot(rows, both_ref[...], preferred_element_type=wide)
        hidden = jnp.where(fresh, jax.nn.silu(inner[:, :part]) * inner[:, part:], 0.0)
        hidden = hidden.astype(jnp.bfloat16)
        if len(downs_ref.shape) == 3:
            for i in range(downs_ref.shape[0]):
                piece = jnp.dot(hidden, downs_ref[i], preferred_element_type=wide)
                part_ref[k, :, :, :, i * narrow : (i + 1) * narrow] = piece.astype(
                    jnp.bfloat16
                ).reshape(nx, nc, share, narrow)
        else:
            piece = jnp.dot(hidden, downs_ref[...], preferred_element_type=wide)
            part_ref[k] = piece.astype(jnp.bfloat16).reshape(nx, nc, share, -1)
        for l in range(1, nc):
            for i in range(nx):
                over_c[k, i, l] = send(
                    part_ref.at[k, i, lax.rem(c + l, nc)],
                    got_c.at[k, i, l - 1],
                    plan.device(plan.shifted(here, "c", l)),
                    c_s.at[k, i, l],
                    c_r.at[k, i, l],
                )

    def fold_c(k):
        for i in range(nx):
            total = part_ref[k, i, c].astype(wide)
            for l in range(1, nc):
                over_c[k, i, l].wait_recv()
                total += got_c[k, i, l - 1].astype(wide)
            sum_c[k, i] = total.astype(jnp.bfloat16)
        for j in range(1, nx):
            over_x[k, j] = send(
                sum_c.at[k, lax.rem(x + j, nx)],
                got_x.at[k, j - 1],
                plan.device(plan.shifted(here, "x", j)),
                x_s.at[k, j],
                x_r.at[k, j],
            )

    def fold_x(k):
        total = sum_c[k, x].astype(wide)
        for j in range(1, nx):
            over_x[k, j].wait_recv()
            total += got_x[k, j - 1].astype(wide)
        if k == 0:
            mid_ref[...] += total
            return
        sum_x[k - 1] = total.astype(jnp.bfloat16)
        back[k] = send(
            sum_x.at[k - 1],
            got_z.at[k - 1],
            plan.device(plan.shifted(here, "z", -k)),
            z_s.at[k],
            z_r.at[k],
        )

    for k in range(nz):
        hn.relay_on(k)
        if k + 1 < nz:
            hn.relay(k + 1)
        hn.landed(k)
        feed(k)
        if k:
            fold_x(k - 1)
        fold_c(k)
    fold_x(nz - 1)
    total = mid_ref[...]
    for k in range(1, nz):
        back[k].wait_recv()
        total += got_z[k - 1].astype(wide)
    o_ref[...] = total.astype(jnp.bfloat16)
    kv.finish()
    hn.finish()
    for copies in (over_z, over_r, over_c, over_x, back):
        for copy in copies.values():
            copy.wait_send()
    for copy in swaps:
        copy.wait_send()


def front(plan, heads, part, kv, qp, qr, wk, wv, wo, resid, gain, gate, up, down, ident):
    nz, nr, nx, nc, tp = plan.z, plan.r, plan.x, plan.c, plan.tp
    share, width = resid.shape
    tok = qp.shape[0]
    dma = pltpu.SemaphoreType.DMA
    vmem = pl.BlockSpec(memory_space=pltpu.VMEM)

    def sems(a, b, c):
        return [dma((a,)), dma((a,)), dma((a, b)), dma((a, b)), dma((a, b, c)), dma((a, b, c))]

    bf = jnp.bfloat16
    narrow = down.shape[1]
    downs = (part, plan.sp * narrow) if narrow % 128 == 0 else (plan.sp, part, narrow)
    return pl.pallas_call(
        functools.partial(front_body, plan, heads, part),
        out_shape=jax.ShapeDtypeStruct((share, width), bf),
        in_specs=[vmem] * 11,
        out_specs=vmem,
        scratch_shapes=[
            pltpu.VMEM((share, width), jnp.float32),
            pltpu.VMEM((nz * tp, share, width), bf),
            pltpu.VMEM((plan.sp * gate.shape[0], 2 * part), bf),
            pltpu.VMEM(downs, bf),
            pltpu.VMEM((nz * nr * nc,) + kv.shape, bf),
            pltpu.VMEM((tok, heads * VDIM), bf),
            pltpu.VMEM((tp, share, width), bf),
            pltpu.VMEM((tp, share, width), bf),
            pltpu.VMEM((share, width), bf),
            pltpu.VMEM((nz, nx, nc, share, width), bf),
            pltpu.VMEM((nz, nx, max(nc - 1, 1), share, width), bf),
            pltpu.VMEM((nz, nx, share, width), bf),
            pltpu.VMEM((nz, max(nx - 1, 1), share, width), bf),
            pltpu.VMEM((max(nz - 1, 1), share, width), bf),
            pltpu.VMEM((max(nz - 1, 1), share, width), bf),
            *sems(nz, nr, nc),
            *sems(nz, nx, nc),
            dma((3, nz)),
            dma((3, nz)),
            dma((3, nz, nr)),
            dma((3, nz, nr)),
            dma((tp,)),
            dma((tp,)),
            dma((nz, nx, nc)),
            dma((nz, nx, nc)),
            dma((nz, nx)),
            dma((nz, nx)),
            dma((nz,)),
            dma((nz,)),
            dma((5,)),
        ],
        compiler_params=pltpu.CompilerParams(
            collective_id=ident, has_side_effects=True, vmem_limit_bytes=62 * 1024 * 1024
        ),
    )(kv, qp, qr, wk, wv, wo, resid, gain, gate, up, down)


def shards(
    plan,
    resid_in,
    query_latent,
    kv_latent,
    rotary_key,
    query_gain,
    kv_gain,
    w_query_plain,
    w_query_rotary,
    w_key_plain,
    w_value,
    w_output,
    ffn_gain,
    w_gate,
    w_up,
    w_down,
):
    tok = resid_in.shape[0]
    heads_dev = w_query_plain.shape[1] // NOPE
    nz = plan.z
    hidden_dev = w_gate.shape[1]
    part = min(-(-hidden_dev // (nz * 128)) * 128, hidden_dev)

    offset = lax.axis_index("sp") * tok
    position = (offset + jnp.arange(tok, dtype=jnp.int32)).astype(jnp.float32)
    freq = 10000.0 ** (-jnp.arange(0, ROPE, 2, dtype=jnp.float32) / ROPE)
    angle = position[:, None] * freq[None, :]
    cosine = jnp.cos(angle)
    sine = jnp.sin(angle)
    kv_norm = normed(kv_latent, kv_gain).astype(jnp.bfloat16)
    key_rot = rotate(rotary_key.astype(jnp.float32), cosine, sine).astype(jnp.bfloat16)
    piece = tok // plan.c
    packed = lax.dynamic_slice_in_dim(
        jnp.concatenate([kv_norm, key_rot], axis=1),
        lax.rem(lax.axis_index("tp"), plan.c) * piece,
        piece,
        0,
    )
    q_norm = normed(query_latent, query_gain).astype(jnp.bfloat16)
    q_plain = (
        jnp.dot(q_norm, w_query_plain, preferred_element_type=jnp.float32)
        .astype(jnp.bfloat16)
    )
    q_raw = jnp.dot(q_norm, w_query_rotary, preferred_element_type=jnp.float32).reshape(
        tok, heads_dev, ROPE
    )
    q_rot = rotate(q_raw, cosine[:, None, :], sine[:, None, :]).astype(jnp.bfloat16)
    share = tok // plan.tp
    own_start = lax.axis_index("tp") * share
    return front(
        plan,
        heads_dev,
        part,
        packed,
        q_plain,
        jnp.transpose(q_rot, (1, 0, 2)),
        w_key_plain,
        w_value,
        w_output,
        lax.dynamic_slice_in_dim(resid_in, own_start, share, 0),
        ffn_gain[None, :],
        w_gate,
        w_up,
        w_down,
        1,
    )


def solution(mesh):
    plan = Plan(mesh.shape["sp"], mesh.shape["tp"])
    return jax.shard_map(
        functools.partial(shards, plan),
        mesh=mesh,
        in_specs=(
            P("sp", None),
            P("sp", None),
            P("sp", None),
            P("sp", None),
            P(),
            P(),
            P(None, "tp"),
            P(None, "tp"),
            P(None, "tp"),
            P(None, "tp"),
            P("tp", None),
            P(),
            P("sp", "tp"),
            P("sp", "tp"),
            P("tp", "sp"),
        ),
        out_specs=P(("sp", "tp"), None),
        check_vma=False,
    )
```

profile of v0, /device:TPU:0, one launch (start us, length us, event | category | flops | bytes accessed | tf_op | source)
XLA Modules:
  0.0 159.3 jit_solution(9742077233646482310)
XLA Ops:
  0.0 0.0 copy-start
  0.0 0.0 copy-start.1
  0.0 0.0 copy-start.3
  0.0 0.0 copy-start.2
  0.0 1.0 copy.20
  1.1 0.6 multiply_cosine_fusion
  1.7 1.1 fusion.3
  2.8 1.1 fusion.5
  3.8 0.8 fusion.7.kv_ref
  4.6 0.0 copy-done.1
  4.6 0.2 fusion
  4.8 0.0 copy-done.3
  4.8 0.0 copy-done.2
  4.8 0.4 fusion.8
  5.2 0.2 copy.24
  5.4 0.2 copy.25
  5.6 0.2 subtract_convert_fusion
  5.8 0.8 maximum_bitcast_fusion.qr_ref
  6.6 0.0 copy-done
  6.6 0.7 constant_dynamic-slice_fusion.resid_ref
  7.4 2.3 %convolution_convert_fusion.qp_ref = bf16[256,512]{1,0:T(8,128)(2,1)} fusion(bf16[768,512]{1,0:T(8,128)(2,1)} %param.21, bf16[256,768]{1,0:T(8,128)(2,1)S(1)} %copy-done.1, f32[768]{0:T(1024)S(1)} %copy-done.3, f32[256]{0:T(256)S(1)} %add_rsqrt_fusion), kind=kOutput, calls=%fused_computation | convolution fusion | flops 202244096 | bytes 1445888 | tf_op jit(solution)/shard_map/dot_general | solution.py:497
  9.6 148.0 %shard_map.145 = bf16[64,2048]{1,0:T(8,128)(2,1)} custom-call(bf16[128,576]{1,0:T(8,128)(2,1)} %fusion.7.kv_ref, bf16[256,512]{1,0:T(8,128)(2,1)} %convolution_convert_fusion.qp_ref, bf16[4,256,64]{2,1,0:T(8,128)(2,1)} %maximum_bitcast_fusion.qr_ref, bf16[512,512]{1,0:T(8,128)(2,1)} %wk_ref.1, bf16[512,512]{1,0:T(8,128)(2,1)} %wv_ref.1, ...), custom_call_target="tpu_custom_call" | custom-call | tf_op jit(solution)/shard_map/pallas_call | solution.py:413
  157.6 1.7 %copy.27 = bf16[64,2048]{1,0:T(8,128)(2,1)} copy(bf16[64,2048]{1,0:T(8,128)(2,1)} %shard_map.145) | data formatting | bytes 524288
  (6 shorter events, 0.1 us)
Async XLA Ops:
  0.0 6.6 %copy-start = (bf16[256,2048]{1,0:T(8,128)(2,1)S(1)}, bf16[256,2048]{1,0:T(8,128)(2,1)}, u32[]{:S(2)}) copy-start(bf16[256,2048]{1,0:T(8,128)(2,1)} %param.15) | copy-start | bytes 3145732
  0.0 4.6 %copy-start.1 = (bf16[256,768]{1,0:T(8,128)(2,1)S(1)}, bf16[256,768]{1,0:T(8,128)(2,1)}, u32[]{:S(2)}) copy-start(bf16[256,768]{1,0:T(8,128)(2,1)} %param.16) | copy-start | bytes 1179652
  0.0 4.8 %copy-start.3 = (f32[768]{0:T(1024)S(1)}, f32[768]{0:T(1024)}, u32[]{:S(2)}) copy-start(f32[768]{0:T(1024)} %param.19) | copy-start | bytes 9220
  0.0 4.8 %copy-start.2 = (bf16[768,256]{1,0:T(8,128)(2,1)S(1)}, bf16[768,256]{1,0:T(8,128)(2,1)}, u32[]{:S(2)}) copy-start(bf16[768,256]{1,0:T(8,128)(2,1)} %param.22) | copy-start | bytes 1179652
where the time goes:
time: 160 us; the launch traced here: 159 us
  Pallas kernels  148 us (92%)
  other arithmetic  4.7 us (3%)
  local copies, waits for them, and re-layouts  3.8 us (2%)
  matrix products  2.66 us (2%)
    pallas_call x1, Pallas kernels, front(): pl.pallas_call(functools.partial(front_body, plan, heads, part), out_shap...  148 us

commit v1 on v0

v1 whole, which is shorter than its diff:
```python
import functools

import jax
import jax.numpy as jnp
from jax import lax
from jax.experimental import pallas as pl
from jax.experimental.pallas import tpu as pltpu
from jax.sharding import PartitionSpec as P

NOPE = 128
ROPE = 64
VDIM = 128
MESH = pl.DeviceIdType.MESH


def normed(values, gain):
    wide = values.astype(jnp.float32)
    return wide * lax.rsqrt(jnp.mean(wide * wide, axis=-1, keepdims=True) + 1e-06) * gain


class Plan:
    def __init__(self, sp, tp):
        self.sp, self.tp = sp, tp
        self.z = 4 if sp % 4 == 0 else 1
        self.r = sp // self.z
        self.c = 2 if tp % 2 == 0 else 1
        self.x = tp // self.c

    def sizes(self):
        return {"z": self.z, "r": self.r, "x": self.x, "c": self.c}

    def here(self):
        s, t = lax.axis_index("sp"), lax.axis_index("tp")
        return {"z": s // self.r, "r": lax.rem(s, self.r), "x": t // self.c, "c": lax.rem(t, self.c)}

    def device(self, at):
        return {"sp": at["z"] * self.r + at["r"], "tp": at["x"] * self.c + at["c"]}

    def shifted(self, at, axis, by):
        size = self.sizes()[axis]
        return {**at, axis: lax.rem(at[axis] + (by % size), size)}

    def far(self):
        return (2, 3, 1) if self.z == 4 else ()

    def partner(self, at, m):
        z = at["z"]
        if m == 1:
            z = z + 1 - 2 * lax.rem(z, 2)
        elif m == 2:
            z = lax.rem(z + 2, 4)
        elif m == 3:
            z = 3 - z
        return {**at, "z": z}


def front_body(
    plan,
    heads,
    part,
    ql_ref,
    kvl_ref,
    rk_ref,
    qg_ref,
    kg_ref,
    cos_ref,
    sin_ref,
    gain_ref,
    wqp_hbm,
    wqr_hbm,
    wk_hbm,
    wv_hbm,
    wo_hbm,
    resid_hbm,
    gate_ref,
    up_ref,
    down_ref,
    o_ref,
    mid_ref,
    hn_ref,
    both_ref,
    downs_ref,
    packed,
    attn,
    wqp_ref,
    wqr_ref,
    wk_ref,
    wv_ref,
    wo_ref,
    resid_ref,
    qcat,
    proj_ref,
    outp,
    swap_c,
    swap_s,
    swap_x,
    hidden,
    part_ref,
    got_c,
    sum_c,
    got_x,
    sum_x,
    got_z,
    kz_s,
    kz_r,
    ky_s,
    ky_r,
    kx_s,
    kx_r,
    kc_s,
    kc_r,
    wz_s,
    wz_r,
    wy_s,
    wy_r,
    sc_s,
    sc_r,
    sx_s,
    sx_r,
    hz_s,
    hz_r,
    hx_s,
    hx_r,
    hc_s,
    hc_r,
    fc_s,
    fc_r,
    fx_s,
    fx_r,
    fz_s,
    fz_r,
    local,
):
    here = plan.here()
    nz, nr, nx, nc, tp = plan.z, plan.r, plan.x, plan.c, plan.tp
    far = plan.far()
    z, r, x, c = here["z"], here["r"], here["x"], here["c"]
    latent = wk_ref.shape[0]
    depth, full = gate_ref.shape
    narrow = down_ref.shape[1]
    tok = ql_ref.shape[0]
    share = tok // tp
    sp_here, tp_here = lax.axis_index("sp"), lax.axis_index("tp")
    wide, bf = jnp.float32, jnp.bfloat16
    f32 = wide
    waits = []

    def drain():
        while waits:
            waits.pop().wait_send()

    def peer(axis, by):
        return plan.device(plan.shifted(here, axis, by))

    def zpeer(m):
        return plan.device(plan.partner(here, m))

    def zof(m):
        return plan.partner(here, m)["z"]

    barrier = pltpu.get_barrier_semaphore()
    peers = [zpeer(m) for m in far]
    for axis, size in (("r", nr), ("x", nx), ("c", nc)):
        peers += [peer(axis, k) for k in range(1, size)]
    for to in peers:
        pl.semaphore_signal(barrier, inc=1, device_id=to, device_id_type=MESH)

    loads = [
        (wqp_hbm, wqp_ref),
        (wqr_hbm, wqr_ref),
        (wk_hbm, wk_ref),
        (wv_hbm, wv_ref),
        (wo_hbm, wo_ref),
        (resid_hbm.at[pl.ds(pl.multiple_of(tp_here * share, share), share)], resid_ref),
    ]
    loads = [pltpu.make_async_copy(s, d, local.at[i]) for i, (s, d) in enumerate(loads)]
    for copy in loads:
        copy.start()

    def send(src, dst, device, sem_s, sem_r):
        copy = pltpu.make_async_remote_copy(
            src_ref=src,
            dst_ref=dst,
            send_sem=sem_s,
            recv_sem=sem_r,
            device_id=device,
            device_id_type=MESH,
        )
        copy.start()
        waits.append(copy)
        return copy

    pair = 2 * ROPE
    lane = lax.broadcasted_iota(jnp.int32, (1, pair), 1)
    first = lax.rem(lane, ROPE) < ROPE // 2

    def rotated(v):
        other = jnp.where(first, pltpu.roll(v, pair - ROPE // 2, 1), pltpu.roll(v, ROPE // 2, 1))
        return (v * cos_ref[...] + other * sin_ref[...]).astype(bf)

    def block_of(at):
        return at["z"] * nr + at["r"]

    with jax.named_scope("kvprep"):
        lat = normed(kvl_ref[...], kg_ref[...][None, :]).astype(bf)
        raw = rk_ref[...].astype(f32)
        rot = rotated(jnp.concatenate([raw, raw], axis=0).T)
        for i in range(tp):
            rows = slice(i * share, (i + 1) * share)
            packed[sp_here, i % nc, i // nc, :, :latent] = lat[rows]
            packed[sp_here, i % nc, i // nc, :, latent:] = rot[rows]

    with jax.named_scope("barrier"):
        pl.semaphore_wait(barrier, len(peers))

    kz, ky, kx, kc = {}, {}, {}, {}

    def kv_at(m, j):
        return block_of(plan.shifted(plan.partner(here, m), "r", -j))

    def kv_y(m):
        q = packed.at[kv_at(m, 0), c]
        q = q if m == 0 else q.at[x]
        for j in range(1, nr):
            ky[m, j] = send(q, q, peer("r", j), ky_s.at[m, j], ky_r.at[m, j])

    def kv_x(m, j):
        for l in range(1, nx):
            q = packed.at[kv_at(m, j), c, x]
            kx[m, j, l] = send(q, q, peer("x", l), kx_s.at[m, j, l], kx_r.at[m, j, l])

    def kv_c(m, j):
        for l in range(1, nx):
            if (m, j, l) in kx:
                kx[m, j, l].wait_recv()
        for l in range(1, nc):
            q = packed.at[kv_at(m, j), c]
            kc[m, j, l] = send(q, q, peer("c", l), kc_s.at[m, j, l], kc_r.at[m, j, l])

    own = packed.at[sp_here, c]
    for m in far:
        q = own if m == 1 else own.at[x]
        kz[m] = send(q, q, zpeer(m), kz_s.at[m], kz_r.at[m])
    kv_y(0)

    def window(index):
        return pl.multiple_of(jnp.minimum(index * part, full - part), 128)

    def targets(sp):
        rows = pl.ds(pl.multiple_of(sp * depth, depth), depth)
        if len(downs_ref.shape) == 3:
            downs = downs_ref.at[sp]
        else:
            downs = downs_ref.at[:, pl.ds(pl.multiple_of(sp * narrow, 128), narrow)]
        return [
            both_ref.at[rows, pl.ds(0, part)],
            both_ref.at[rows, pl.ds(part, part)],
            downs,
        ]

    def sources(index):
        lanes = pl.ds(window(index), part)
        return [gate_ref.at[:, lanes], up_ref.at[:, lanes], down_ref.at[lanes, :]]

    over_z, over_r = {}, {}
    streams = []
    mine = []

    for w in range(3):
        for m in far:
            over_z[w, m] = pltpu.make_async_remote_copy(
                src_ref=sources(zof(m))[w],
                dst_ref=targets(sp_here)[w],
                send_sem=wz_s.at[w, m],
                recv_sem=wz_r.at[w, m],
                device_id=zpeer(m),
                device_id_type=MESH,
            )

    inside = lax.rem(z, 3) != 0
    outside = lax.rem(z, 3) == 0

    def spread(w, *ms):
        for m in ms:
            if m in far:
                over_z[w, m].start()

    def spread_if(when, w, *ms):
        @pl.when(when)
        def _():
            spread(w, *ms)

    def forward(w, m):
        dst = targets(kv_at(m, 0))[w]
        src = dst if m else sources(z)[w]
        if m:
            over_z[w, m].wait_recv()
        for j in range(1, nr):
            over_r[w, m, j] = send(src, dst, peer("r", j), wy_s.at[w, m, j], wy_r.at[w, m, j])
            streams.append(waits.pop())

    for w in range(3):
        mine.append(pltpu.make_async_copy(sources(z)[w], targets(sp_here)[w], local.at[8 + w]))
        mine[-1].start()

    early = len(proj_ref.shape) == 3

    def project(sp):
        if early:
            kv = packed[sp, :, :, :, :latent].reshape(tok, latent)
            for i, w_ref in enumerate((wk_ref, wv_ref)):
                out = jnp.dot(kv, w_ref[...], preferred_element_type=f32)
                proj_ref[i, pl.ds(pl.multiple_of(sp * tok, tok), tok), :] = out.astype(bf)

    with jax.named_scope("qprep"):
        qn = normed(ql_ref[...], qg_ref[...][None, :]).astype(bf)
        loads[0].wait()
        loads[1].wait()
        plain = jnp.dot(qn, wqp_ref[...], preferred_element_type=f32).astype(bf)
        turned = jnp.dot(qn, wqr_ref[...], preferred_element_type=f32)
        for h in range(heads):
            p = h // 2 * pair
            both = rotated(turned[:, p : p + pair])
            keep = (lane >= ROPE) if h % 2 else (lane < ROPE)
            qcat[h, :, :NOPE] = plain[:, h * NOPE : (h + 1) * NOPE]
            qcat[h, :, NOPE:] = jnp.where(keep, both.astype(f32), 0.0).astype(bf)

    loads[2].wait()
    loads[3].wait()
    with jax.named_scope("projown"):
        project(sp_here)
    with jax.named_scope("kvz"):
        for m in far:
            kz[m].wait_recv()
            kv_y(m)
            if m == 1:
                kv_c(m, 0)
            else:
                kv_x(m, 0)
    spread(0, *far)
    spread_if(inside, 1, 2, 1)
    spread_if(outside, 1, 3)
    spread_if(inside, 1, 3)
    spread_if(outside, 1, 2, 1)
    near = [(0, j) for j in range(1, nr)] + [(1, 0)][: len(far)]
    rest = [(m, 0) for m in far if m != 1]
    late = [(m, j) for j in range(1, nr) for m in far]

    def landed(keys):
        for m, j in keys:
            for l in range(1, nc):
                kc[m, j, l].wait_recv()
            project(kv_at(m, j))

    with jax.named_scope("kvy"):
        for j in range(1, nr):
            ky[0, j].wait_recv()
            kv_c(0, j)
        for m, j in late:
            ky[m, j].wait_recv()
            kv_x(m, j)
    with jax.named_scope("near"):
        landed(near)
    with jax.named_scope("kvc"):
        for m, j in rest:
            kv_c(m, j)
        with jax.named_scope("kvcl"):
            landed(rest)
    with jax.named_scope("kvlate"):
        for key in late:
            kv_c(*key)
        for w in range(3):
            forward(w, 0)
        landed(late)

    scale = (NOPE + ROPE) ** (-0.5)
    count = plan.sp * tok

    def transposed(left, right):
        return lax.dot_general(
            left, right, (((1,), (1,)), ((), ())), preferred_element_type=f32
        )

    def head(h):
        lanes = pl.ds(pl.multiple_of(h * NOPE, NOPE), NOPE)
        rot = packed[:, :, :, :, latent:].reshape(count, pair)
        if early:
            plain, vals = proj_ref[0, :, lanes], proj_ref[1, :, lanes]
        else:
            kv = packed[:, :, :, :, :latent].reshape(count, latent)
            weights = jnp.concatenate([wk_ref[:, lanes], wv_ref[:, lanes]], axis=1)
            mixed = jnp.dot(kv, weights, preferred_element_type=f32).astype(bf)
            plain, vals = mixed[:, :NOPE], mixed[:, NOPE:]
        score = transposed(qcat[h], jnp.concatenate([plain, rot], axis=1)) * scale
        weight = jnp.exp(score - jnp.max(score, axis=-1, keepdims=True))
        total = jnp.sum(weight, axis=-1, keepdims=True)
        value = jnp.dot(weight.astype(bf), vals, preferred_element_type=f32)
        attn[:, lanes] = (value / total).astype(bf)

    todo = [(w, m) for w in range(2) for m in far]

    def pump(n):
        for _ in range(n):
            if todo:
                forward(*todo.pop(0))

    @pl.loop(0, heads)
    def _(h):
        with jax.named_scope("head"):
            head(h)

    with jax.named_scope("pump0"):
        pump(PUMPS[0])
    with jax.named_scope("outproj"):
        loads[4].wait()
        loads[5].wait()
        term = jnp.dot(attn[...], wo_ref[...], preferred_element_type=f32).astype(bf)
        for i in range(tp):
            outp[i % nc, i // nc] = term[i * share : (i + 1) * share]
    swaps_c = [
        send(
            outp.at[lax.rem(c + l, nc)], swap_c.at[l - 1], peer("c", l), sc_s.at[l], sc_r.at[l]
        )
        for l in range(1, nc)
    ]
    with jax.named_scope("swapc"):
        for copy in swaps_c:
            copy.wait_recv()

    def folded(i):
        total = outp[c, i].astype(f32)
        for l in range(1, nc):
            total += swap_c[l - 1, i].astype(f32)
        return total

    swaps_x = []
    for l in range(1, nx):
        i = lax.rem(x + l, nx)
        swap_s[l - 1] = folded(i).astype(bf)
        swaps_x.append(
            send(swap_s.at[l - 1], swap_x.at[l - 1], peer("x", l), sx_s.at[l], sx_r.at[l])
        )
    mid = resid_ref[...].astype(f32) + folded(x)
    with jax.named_scope("pumpA"):
        pump(PUMPS[1])
    drain()
    with jax.named_scope("swapx"):
        for l, copy in enumerate(swaps_x):
            copy.wait_recv()
            mid += swap_x[l].astype(f32)
    mid_ref[...] = mid
    hn_ref[z, c, x] = (
        mid * lax.rsqrt(jnp.mean(mid * mid, axis=-1, keepdims=True) + 1e-06) * gain_ref[...][None, :]
    ).astype(bf)

    hz, hx, hc = {}, {}, {}
    order = (0,) + tuple(range(1, nz))
    half = z // 2
    origin = (z, z + 1 - 2 * lax.rem(z, 2), 2 - half, 3 - 3 * half)[:nz]
    inner_z = inside

    def hn_z(k, device, at):
        q = hn_ref.at[origin[k], c, x]
        return pltpu.make_async_remote_copy(
            src_ref=q,
            dst_ref=q,
            send_sem=hz_s.at[k, at],
            recv_sem=hz_r.at[at],
            device_id=device,
            device_id_type=MESH,
        )

    def hn_send(copy, when=None):
        @pl.when(inner_z if when is None else when)
        def _():
            copy.start()

        hops.append(copy)

    hops = []

    def hn_x(k):
        q = hn_ref.at[origin[k], c, x]
        for l in range(1, nx):
            hx[k, l] = send(q, q, peer("x", l), hx_s.at[k, l], hx_r.at[k, l])

    def hn_c(k):
        for l in range(1, nx):
            hx[k, l].wait_recv()
        q = hn_ref.at[origin[k], c]
        for l in range(1, nc):
            hc[k, l] = send(q, q, peer("c", l), hc_s.at[k, l], hc_r.at[k, l])

    if nz > 1:
        direct = hn_z(0, zpeer(1), 1)
        direct.start()
        waits.append(direct)
        hn_send(hn_z(0, zpeer(3), 2))
    hn_x(0)
    if nz > 1:
        with jax.named_scope("hn1"):
            hn_z(1, zpeer(1), 1).wait_recv()
            hn_send(hn_z(1, zpeer(3), 3))
            hn_x(1)
        spread_if(inside, 2, 3)
        with jax.named_scope("pumpB"):
            pump(PUMPS[2])
        hn_c(0)
        with jax.named_scope("hn2"):
            hn_z(2, zpeer(1), 2).wait_recv()
            hn_send(hn_z(2, zpeer(1), 2))
            hn_x(2)
        spread_if(outside, 2, 2, 1)
        hn_c(1)
        with jax.named_scope("hn3"):
            hn_z(3, zpeer(1), 3).wait_recv()
            hn_send(hn_z(3, zpeer(1), 3))
            hn_x(3)
        spread_if(inside, 2, 2, 1)
        spread_if(outside, 2, 3)
    else:
        hn_c(0)
    with jax.named_scope("pumpC"):
        pump(9)
    todo += [(2, m) for m in far]
    for k in order[2:]:
        with jax.named_scope(f"hnc{k}"):
            hn_c(k)
    with jax.named_scope("gateup"):
        for w in range(2):
            mine[w].wait()
            for m in (0,) + far:
                for j in range(1, nr):
                    over_r[w, m, j].wait_recv()

    place = z * part
    lanes = lax.broadcasted_iota(jnp.int32, (1, part), 1)
    fresh = lanes >= place - jnp.minimum(place, full - part)

    def inner(k):
        for l in range(1, nc):
            hc[k, l].wait_recv()
        rows = hn_ref[origin[k]].reshape(tp * share, -1)
        both = jnp.dot(rows, both_ref[...], preferred_element_type=f32)
        value = jnp.where(fresh, jax.nn.silu(both[:, :part]) * both[:, part:], 0.0)
        hidden[origin[k]] = value.astype(bf)

    for k in order:
        with jax.named_scope(f"inner{k}"):
            inner(k)
    order = (0,) + far
    pump(PUMPS[3])

    over_c, over_x, back = {}, {}, {}
    group = nr * narrow

    def feed(m):
        if m == 0:
            mine[2].wait()
        for j in range(1, nr):
            over_r[2, m, j].wait_recv()
        rows = hidden[...].reshape(nz * tp * share, part)

        def keep(piece, columns):
            piece = piece.astype(bf).reshape(nz, nc, nx, share, -1)
            for i in range(nc):
                part_ref[m, i, :, :, :, columns] = piece[:, i]

        if len(downs_ref.shape) == 3:
            for i in range(nr):
                piece = jnp.dot(rows, downs_ref[zof(m) * nr + i], preferred_element_type=f32)
                keep(piece, slice(i * narrow, (i + 1) * narrow))
        else:
            columns = pl.ds(pl.multiple_of(zof(m) * group, 128), group)
            keep(jnp.dot(rows, downs_ref[:, columns], preferred_element_type=f32), slice(None))
        for l in range(1, nc):
            over_c[m, l] = send(
                part_ref.at[m, lax.rem(c + l, nc)],
                got_c.at[m, l - 1],
                peer("c", l),
                fc_s.at[m, l],
                fc_r.at[m, l],
            )

    def fold_c(m):
        for l in range(1, nc):
            over_c[m, l].wait_recv()
        for k in range(1, nx + 1):
            i = lax.rem(x + k, nx)
            total = part_ref[m, c, :, i].astype(f32)
            for l in range(1, nc):
                total += got_c[m, l - 1, :, i].astype(f32)
            sum_c[m, i] = total.astype(bf)
            if k < nx:
                over_x[m, k] = send(
                    sum_c.at[m, i], got_x.at[m, k - 1], peer("x", k), fx_s.at[m, k], fx_r.at[m, k]
                )

    def columns_of(m):
        return pl.ds(pl.multiple_of(zof(m) * group, 128), group)

    def fold_x(m):
        for k in range(1, nx):
            over_x[m, k].wait_recv()
        for p in far + (0,):
            total = sum_c[m, x, zof(p)].astype(f32)
            for k in range(1, nx):
                total += got_x[m, k - 1, zof(p)].astype(f32)
            if p == 0:
                mid_ref[:, columns_of(m)] += total
                continue
            sum_x[m, p] = total.astype(bf)
            there = m ^ p
            back[there, p] = send(
                sum_x.at[m, p], got_z.at[there, p], zpeer(p), fz_s.at[m, p], fz_r.at[there, p]
            )

    def close(m):
        total = mid_ref[:, columns_of(m)]
        for p in far:
            back[m, p].wait_recv()
            total += got_z[m, p].astype(f32)
        o_ref[:, columns_of(m)] = total.astype(bf)

    plain = ((feed, 0), (pump, 1), (fold_c, 0), (pump, 1), (feed, 1), (fold_c, 1), (pump, 1))
    plain += ((fold_x, 0), (feed, 2), (fold_c, 2), (fold_x, 1), (feed, 3), (fold_c, 3))
    def settle(i):
        for copy in over_z.values():
            copy.wait_send()
        for copy in hops:

            @pl.when(inner_z)
            def _():
                copy.wait_send()

        last = {id(copy) for copy in back.values()}
        held = streams + [copy for copy in waits if id(copy) not in last]
        waits[:] = [copy for copy in waits if id(copy) in last]
        for copy in held:
            copy.wait_send()

    plain += ((fold_x, 2), (settle, 0), (fold_x, 3), (close, 0), (close, 1), (close, 2), (close, 3))
    for stage, i in plain:
        with jax.named_scope(f"{stage.__name__}{i}"):
            if stage is pump:
                pump(i)
            elif i < len(order):
                stage(order[i])
    drain()


PUMPS = (1, 2, 3, 0)


def front(plan, heads, part, args):
    nz, nr, nx, nc, tp = plan.z, plan.r, plan.x, plan.c, plan.tp
    ql, kvl = args[0], args[1]
    wqp, wqr, wk, wv, wo, resid, gate, up, down = args[8:]
    tok, width = resid.shape
    share = tok // tp
    dma = pltpu.SemaphoreType.DMA
    vmem = pl.BlockSpec(memory_space=pltpu.VMEM)
    hbm = pl.BlockSpec(memory_space=pl.ANY)
    bf = jnp.bfloat16
    narrow = down.shape[1]
    group = nr * narrow
    downs = (part, plan.sp * narrow) if narrow % 128 == 0 else (plan.sp, part, narrow)
    proj = (2, plan.sp * tok, heads * NOPE)
    proj = pltpu.VMEM(proj if 4 * proj[1] * proj[2] < 2**23 + 1 else (8, 128), bf)
    more_c, more_x = max(nc - 1, 1), max(nx - 1, 1)
    sizes = [(nz,), (nz, nr), (nz, nr, nx), (nz, nr, nc), (3, nz), (3, nz, nr), (nc,), (nx,)]
    sems = [dma(size) for size in sizes for _ in range(2)]
    sems += [dma((2 * nz, 4)), dma((4,))]
    sizes = [(nz, nx), (nz, nc), (nz, nc), (nz, nx), (nz, nz)]
    sems += [dma(size) for size in sizes for _ in range(2)]
    return pl.pallas_call(
        functools.partial(front_body, plan, heads, part),
        out_shape=jax.ShapeDtypeStruct((share, width), bf),
        in_specs=[vmem] * 8 + [hbm] * 9,
        out_specs=vmem,
        scratch_shapes=[
            pltpu.VMEM((share, width), jnp.float32),
            pltpu.VMEM((nz, nc, nx, share, width), bf),
            pltpu.VMEM((plan.sp * gate.shape[0], 2 * part), bf),
            pltpu.VMEM(downs, bf),
            pltpu.VMEM((plan.sp, nc, nx, share, kvl.shape[1] + 2 * ROPE), bf),
            pltpu.VMEM((tok, heads * VDIM), bf),
            pltpu.VMEM(wqp.shape, bf),
            pltpu.VMEM(wqr.shape, bf),
            pltpu.VMEM(wk.shape, bf),
            pltpu.VMEM(wv.shape, bf),
            pltpu.VMEM(wo.shape, bf),
            pltpu.VMEM((share, width), bf),
            pltpu.VMEM((heads, tok, NOPE + 2 * ROPE), bf),
            proj,
            pltpu.VMEM((nc, nx, share, width), bf),
            pltpu.VMEM((more_c, nx, share, width), bf),
            pltpu.VMEM((more_x, share, width), bf),
            pltpu.VMEM((more_x, share, width), bf),
            pltpu.VMEM((nz, tp * share, part), bf),
            pltpu.VMEM((nz, nc, nz, nx, share, group), bf),
            pltpu.VMEM((nz, more_c, nz, nx, share, group), bf),
            pltpu.VMEM((nz, nx, nz, share, group), bf),
            pltpu.VMEM((nz, more_x, nz, share, group), bf),
            pltpu.VMEM((nz, nz, share, group), bf),
            pltpu.VMEM((nz, nz, share, group), bf),
            *sems,
            dma((11,)),
        ],
        compiler_params=pltpu.CompilerParams(
            collective_id=1, has_side_effects=True, vmem_limit_bytes=62 * 1024 * 1024
        ),
    )(*args)


def shards(
    plan,
    resid_in,
    query_latent,
    kv_latent,
    rotary_key,
    query_gain,
    kv_gain,
    w_query_plain,
    w_query_rotary,
    w_key_plain,
    w_value,
    w_output,
    ffn_gain,
    w_gate,
    w_up,
    w_down,
):
    tok = resid_in.shape[0]
    heads_dev = w_query_plain.shape[1] // NOPE
    hidden_dev = w_gate.shape[1]
    part = min(-(-hidden_dev // (plan.z * 128)) * 128, hidden_dev)

    offset = lax.axis_index("sp") * tok
    position = (offset + jnp.arange(tok, dtype=jnp.int32)).astype(jnp.float32)
    lane = lax.broadcasted_iota(jnp.int32, (1, 2 * ROPE), 1)
    index = lax.rem(lane, ROPE // 2) * 2
    freq = 10000.0 ** (-index.astype(jnp.float32) / ROPE)
    angle = position[:, None] * freq
    sign = jnp.where(lax.rem(lane, ROPE) < ROPE // 2, -1.0, 1.0)
    return front(
        plan,
        heads_dev,
        part,
        (
            query_latent,
            kv_latent,
            jnp.transpose(rotary_key),
            query_gain,
            kv_gain,
            jnp.cos(angle),
            jnp.sin(angle) * sign,
            ffn_gain,
            w_query_plain,
            w_query_rotary,
            w_key_plain,
            w_value,
            w_output,
            resid_in,
            w_gate,
            w_up,
            w_down,
        ),
    )


def solution(mesh):
    plan = Plan(mesh.shape["sp"], mesh.shape["tp"])
    return jax.shard_map(
        functools.partial(shards, plan),
        mesh=mesh,
        in_specs=(
            P("sp", None),
            P("sp", None),
            P("sp", None),
            P("sp", None),
            P(),
            P(),
            P(None, "tp"),
            P(None, "tp"),
            P(None, "tp"),
            P(None, "tp"),
            P("tp", None),
            P(),
            P("sp", "tp"),
            P("sp", "tp"),
            P("tp", "sp"),
        ),
        out_specs=P(("sp", "tp"), None),
        check_vma=False,
    )
```

time: 160 us -> 121 us (0.76)
  Pallas kernels: 148 us -> 118 us
  other arithmetic: 4.7 us -> 1.26 us
  matrix products: 2.66 us -> 0 us
  local copies, waits for them, and re-layouts: 3.8 us -> 1.67 us
    pallas_call x1, Pallas kernels: 148 us -> 118 us  [front(): pl.pallas_call(functools.partial(front_body, plan, heads, part), out_shap...]
    dot_general x2 -> x0, matrix products: 2.66 us -> none  [the longest x1 2.25 us: shards(): jnp.dot(q_norm, w_query_plain, preferred_element_type=jnp.float32)]
where the time goes in v1:
time: 121 us
  Pallas kernels  118 us (98%)
  local copies, waits for them, and re-layouts  1.67 us (1%)
  other arithmetic  1.26 us (1%)
    pallas_call x1, Pallas kernels, front(): pl.pallas_call(functools.partial(front_body, plan, heads, part), out_shap...  118 us

profile of v1, /device:TPU:0, one launch (start us, length us, event | category | flops | bytes accessed | tf_op | source)
XLA Modules:
  0.0 120.9 jit_solution(17902595574235733902)
XLA Ops:
  0.0 1.2 %fusion = (f32[256,128]{1,0:T(8,128)}, f32[256,128]{1,0:T(8,128)}) fusion(f32[128]{0:T(128)S(1)} %get-tuple-element.7, f32[128]{0:T(128)S(1)} %get-tuple-element.8, f32[256]{0:T(256)S(1)} %add_convert_fusion), kind=kLoop, calls=%fused_computation.2 | loop fusion | flops 65536 | bytes 264192 | tf_op jit(solution)/shard_map/mul | solution.py:757
  1.3 118.0 %shard_map.145 = bf16[64,2048]{1,0:T(8,128)(2,1)} custom-call(bf16[256,768]{1,0:T(8,128)(2,1)} %ql_ref.1, bf16[256,512]{1,0:T(8,128)(2,1)} %kvl_ref.1, bf16[64,256]{1,0:T(8,128)(2,1)} %bitcast.1, f32[768]{0:T(1024)} %qg_ref.1, f32[512]{0:T(512)} %kg_ref.1, f32[256,128]{1,0:T(8,128)} %get-tuple-element.6.cos_ref, f32[256,128]{1,0:T(8,128)} %get-tuple-element.5.sin_ref, ...), custom_call_target="tpu_custom_call" | custom-call | tf_op jit(solution)/shard_map/pallas_call | solution.py:676
  119.3 1.7 %copy.17 = bf16[64,2048]{1,0:T(8,128)(2,1)} copy(bf16[64,2048]{1,0:T(8,128)(2,1)} %shard_map.145) | data formatting | bytes 524288
  (2 shorter events, 0.0 us)

commit v2 on v1

--- a/solution.py
+++ b/solution.py
@@ -58,14 +58,14 @@
     plan,
     heads,
     part,
-    ql_ref,
-    kvl_ref,
-    rk_ref,
-    qg_ref,
-    kg_ref,
-    cos_ref,
-    sin_ref,
-    gain_ref,
+    ql_hbm,
+    kvl_hbm,
+    rk_hbm,
+    qg_hbm,
+    kg_hbm,
+    cos_hbm,
+    sin_hbm,
+    gain_hbm,
     wqp_hbm,
     wqr_hbm,
     wk_hbm,
@@ -82,6 +82,14 @@
     downs_ref,
     packed,
     attn,
+    ql_ref,
+    kvl_ref,
+    rk_ref,
+    qg_ref,
+    kg_ref,
+    cos_ref,
+    sin_ref,
+    gain_ref,
     wqp_ref,
     wqr_ref,
     wk_ref,
@@ -99,8 +107,9 @@
     got_c,
     sum_c,
     got_x,
-    sum_x,
+    sum_z,
     got_z,
+    done,
     kz_s,
     kz_r,
     ky_s,
@@ -165,6 +174,20 @@
     for to in peers:
         pl.semaphore_signal(barrier, inc=1, device_id=to, device_id_type=MESH)
 
+    smalls = [
+        (kvl_hbm, kvl_ref),
+        (kg_hbm, kg_ref),
+        (rk_hbm, rk_ref),
+        (cos_hbm, cos_ref),
+        (sin_hbm, sin_ref),
+        (ql_hbm, ql_ref),
+        (qg_hbm, qg_ref),
+        (gain_hbm, gain_ref),
+    ]
+    base = 11 + nz
+    smalls = [pltpu.make_async_copy(s, d, local.at[base + i]) for i, (s, d) in enumerate(smalls)]
+    for copy in smalls:
+        copy.start()
     loads = [
         (wqp_hbm, wqp_ref),
         (wqr_hbm, wqr_ref),
@@ -201,6 +224,8 @@
     def block_of(at):
         return at["z"] * nr + at["r"]
 
+    for copy in smalls[:5]:
+        copy.wait()
     with jax.named_scope("kvprep"):
         lat = normed(kvl_ref[...], kg_ref[...][None, :]).astype(bf)
         raw = rk_ref[...].astype(f32)
@@ -222,12 +247,12 @@
         q = packed.at[kv_at(m, 0), c]
         q = q if m == 0 else q.at[x]
         for j in range(1, nr):
-            ky[m, j] = send(q, q, peer("r", j), ky_s.at[m, j], ky_r.at[m, j])
+            ky[m, j] = send(q, q, peer("r", j), ky_s.at[m, j - 1], ky_r.at[m, j - 1])
 
     def kv_x(m, j):
         for l in range(1, nx):
             q = packed.at[kv_at(m, j), c, x]
-            kx[m, j, l] = send(q, q, peer("x", l), kx_s.at[m, j, l], kx_r.at[m, j, l])
+            kx[m, j, l] = send(q, q, peer("x", l), kx_s.at[m, j, l - 1], kx_r.at[m, j, l - 1])
 
     def kv_c(m, j):
         for l in range(1, nx):
@@ -235,7 +260,7 @@
                 kx[m, j, l].wait_recv()
         for l in range(1, nc):
             q = packed.at[kv_at(m, j), c]
-            kc[m, j, l] = send(q, q, peer("c", l), kc_s.at[m, j, l], kc_r.at[m, j, l])
+            kc[m, j, l] = send(q, q, peer("c", l), kc_s.at[m, j, l - 1], kc_r.at[m, j, l - 1])
 
     own = packed.at[sp_here, c]
     for m in far:
@@ -290,13 +315,61 @@
         def _():
             spread(w, *ms)
 
+    def arrange(w, m):
+        dst = targets(kv_at(m, 0))[w]
+        src = dst if m else sources(z)[w]
+        for j in range(1, nr):
+            over_r[w, m, j] = pltpu.make_async_remote_copy(
+                src_ref=src,
+                dst_ref=dst,
+                send_sem=wy_s.at[w, m, j - 1],
+                recv_sem=wy_r.at[w, m, j - 1],
+                device_id=peer("r", j),
+                device_id_type=MESH,
+            )
+            streams.append(over_r[w, m, j])
+
+    def go(w, m):
+        if m:
+            over_z[w, m].wait_recv()
+        for j in range(1, nr):
+            over_r[w, m, j].start()
+
+    def forward(w, m):
+        arrange(w, m)
+        go(w, m)
+
+    for w in range(3):
+        for m in far:
+            over_z[w, m] = pltpu.make_async_remote_copy(
+                src_ref=sources(zof(m))[w],
+                dst_ref=targets(sp_here)[w],
+                send_sem=wz_s.at[w, m],
+                recv_sem=wz_r.at[w, m],
+                device_id=zpeer(m),
+                device_id_type=MESH,
+            )
+
+    inside = lax.rem(z, 3) != 0
+    outside = lax.rem(z, 3) == 0
+
+    def spread(w, *ms):
+        for m in ms:
+            if m in far:
+                over_z[w, m].start()
+
+    def spread_if(when, w, *ms):
+        @pl.when(when)
+        def _():
+            spread(w, *ms)
+
     def forward(w, m):
         dst = targets(kv_at(m, 0))[w]
         src = dst if m else sources(z)[w]
         if m:
             over_z[w, m].wait_recv()
         for j in range(1, nr):
-            over_r[w, m, j] = send(src, dst, peer("r", j), wy_s.at[w, m, j], wy_r.at[w, m, j])
+            over_r[w, m, j] = send(src, dst, peer("r", j), wy_s.at[w, m, j - 1], wy_r.at[w, m, j - 1])
             streams.append(waits.pop())
 
     for w in range(3):
@@ -313,6 +386,8 @@
                 proj_ref[i, pl.ds(pl.multiple_of(sp * tok, tok), tok), :] = out.astype(bf)
 
     with jax.named_scope("qprep"):
+        for copy in smalls[5:]:
+            copy.wait()
         qn = normed(ql_ref[...], qg_ref[...][None, :]).astype(bf)
         loads[0].wait()
         loads[1].wait()
@@ -339,9 +414,7 @@
                 kv_x(m, 0)
     spread(0, *far)
     spread_if(inside, 1, 2, 1)
-    spread_if(outside, 1, 3)
-    spread_if(inside, 1, 3)
-    spread_if(outside, 1, 2, 1)
+    spread_if(outside, 1, 3, 1)
     near = [(0, j) for j in range(1, nr)] + [(1, 0)][: len(far)]
     rest = [(m, 0) for m in far if m != 1]
     late = [(m, j) for j in range(1, nr) for m in far]
@@ -369,7 +442,7 @@
     with jax.named_scope("kvlate"):
         for key in late:
             kv_c(*key)
-        for w in range(3):
+        for w in range(2):
             forward(w, 0)
         landed(late)
 
@@ -397,7 +470,7 @@
         value = jnp.dot(weight.astype(bf), vals, preferred_element_type=f32)
         attn[:, lanes] = (value / total).astype(bf)
 
-    todo = [(w, m) for w in range(2) for m in far]
+    todo = [(0, m) for m in far]
 
     def pump(n):
         for _ in range(n):
@@ -419,7 +492,7 @@
             outp[i % nc, i // nc] = term[i * share : (i + 1) * share]
     swaps_c = [
         send(
-            outp.at[lax.rem(c + l, nc)], swap_c.at[l - 1], peer("c", l), sc_s.at[l], sc_r.at[l]
+            outp.at[lax.rem(c + l, nc)], swap_c.at[l - 1], peer("c", l), sc_s.at[l - 1], sc_r.at[l - 1]
         )
         for l in range(1, nc)
     ]
@@ -438,7 +511,7 @@
         i = lax.rem(x + l, nx)
         swap_s[l - 1] = folded(i).astype(bf)
         swaps_x.append(
-            send(swap_s.at[l - 1], swap_x.at[l - 1], peer("x", l), sx_s.at[l], sx_r.at[l])
+            send(swap_s.at[l - 1], swap_x.at[l - 1], peer("x", l), sx_s.at[l - 1], sx_r.at[l - 1])
         )
     mid = resid_ref[...].astype(f32) + folded(x)
     with jax.named_scope("pumpA"):
@@ -464,7 +537,7 @@
         return pltpu.make_async_remote_copy(
             src_ref=q,
             dst_ref=q,
-            send_sem=hz_s.at[k, at],
+            send_sem=hz_s.at[{(0, 1): 0, (0, 2): 1, (1, 3): 2, (2, 2): 3, (3, 3): 4}.get((k, at), 0)],
             recv_sem=hz_r.at[at],
             device_id=device,
             device_id_type=MESH,
@@ -482,14 +555,54 @@
     def hn_x(k):
         q = hn_ref.at[origin[k], c, x]
         for l in range(1, nx):
-            hx[k, l] = send(q, q, peer("x", l), hx_s.at[k, l], hx_r.at[k, l])
+            hx[k, l] = send(q, q, peer("x", l), hx_s.at[k, l - 1], hx_r.at[k, l - 1])
+
+    for k in order:
+        q = hn_ref.at[origin[k], c]
+        for l in range(1, nc):
+            hc[k, l] = pltpu.make_async_remote_copy(
+                src_ref=q,
+                dst_ref=q,
+                send_sem=hc_s.at[k, l - 1],
+                recv_sem=hc_r.at[k, l - 1],
+                device_id=peer("c", l),
+                device_id_type=MESH,
+            )
+            waits.append(hc[k, l])
 
     def hn_c(k):
         for l in range(1, nx):
             hx[k, l].wait_recv()
-        q = hn_ref.at[origin[k], c]
         for l in range(1, nc):
-            hc[k, l] = send(q, q, peer("c", l), hc_s.at[k, l], hc_r.at[k, l])
+            hc[k, l].start()
+
+    place = z * part
+    lanes = lax.broadcasted_iota(jnp.int32, (1, part), 1)
+    fresh = lanes >= place - jnp.minimum(place, full - part)
+
+    def inner(k):
+        for l in range(1, nc):
+            hc[k, l].wait_recv()
+        rows = hn_ref[origin[k]].reshape(tp * share, -1)
+        both = jnp.dot(rows, both_ref[...], preferred_element_type=f32)
+        value = jnp.where(fresh, jax.nn.silu(both[:, :part]) * both[:, part:], 0.0)
+        hidden[origin[k]] = value.astype(bf)
+
+    def ready():
+        for w in range(2):
+            mine[w].wait()
+            for m in (0,) + far:
+                for j in range(1, nr):
+                    over_r[w, m, j].wait_recv()
+
+    for m in far:
+        arrange(1, m)
+
+    def ups(when, *ms):
+        @pl.when(when)
+        def _():
+            for m in ms:
+                go(1, m)
 
     if nz > 1:
         direct = hn_z(0, zpeer(1), 1)
@@ -498,132 +611,161 @@
         hn_send(hn_z(0, zpeer(3), 2))
     hn_x(0)
     if nz > 1:
+        with jax.named_scope("upsout"):
+            ups(outside, 2, 1, 3)
+            ups(inside, 1)
+    forward(2, 0)
+    if nz > 1:
         with jax.named_scope("hn1"):
             hn_z(1, zpeer(1), 1).wait_recv()
             hn_send(hn_z(1, zpeer(3), 3))
             hn_x(1)
-        spread_if(inside, 2, 3)
-        with jax.named_scope("pumpB"):
-            pump(PUMPS[2])
-        hn_c(0)
+        spread_if(outside, 1, 2)
+        spread_if(outside, 2, 1)
+        spread_if(inside, 1, 3)
+        with jax.named_scope("hnc0"):
+            hn_c(0)
         with jax.named_scope("hn2"):
             hn_z(2, zpeer(1), 2).wait_recv()
             hn_send(hn_z(2, zpeer(1), 2))
             hn_x(2)
-        spread_if(outside, 2, 2, 1)
-        hn_c(1)
+        with jax.named_scope("upsin2"):
+            ups(inside, 2)
+        with jax.named_scope("hnc1"):
+            hn_c(1)
         with jax.named_scope("hn3"):
             hn_z(3, zpeer(1), 3).wait_recv()
             hn_send(hn_z(3, zpeer(1), 3))
             hn_x(3)
-        spread_if(inside, 2, 2, 1)
-        spread_if(outside, 2, 3)
+        spread_if(outside, 2, 2, 3)
+        spread_if(inside, 2, 3)
+        with jax.named_scope("upsin3"):
+            ups(inside, 3)
+        spread_if(inside, 2, 1, 2)
     else:
         hn_c(0)
-    with jax.named_scope("pumpC"):
-        pump(9)
-    todo += [(2, m) for m in far]
-    for k in order[2:]:
-        with jax.named_scope(f"hnc{k}"):
-            hn_c(k)
-    with jax.named_scope("gateup"):
-        for w in range(2):
-            mine[w].wait()
-            for m in (0,) + far:
-                for j in range(1, nr):
-                    over_r[w, m, j].wait_recv()
-
-    place = z * part
-    lanes = lax.broadcasted_iota(jnp.int32, (1, part), 1)
-    fresh = lanes >= place - jnp.minimum(place, full - part)
-
-    def inner(k):
+
+    group = nr * narrow
+    halves = 2 if nz > 1 else 1
+    deep = nz // halves
+    inside_i = jnp.minimum(lax.rem(z, 3), 1)
+    groups = origin
+    sender = (0,) + ((1, 2 + inside_i, 3 - inside_i) if nz > 1 else ())
+    bases = (2 * half, 2 - 2 * half)[:halves] if nz > 1 else (0,)
+    landing = {1: ((1, 0, 2, 3),) * 2, 2: ((3, 2, 0, 1), (2, 3, 1, 0)), 3: ((3, 2, 1, 0), (2, 3, 0, 1))}
+    away = []
+    over_c, over_x, down_r, back = {}, {}, {}, {}
+
+    def remote(src, dst, device, sem_s, sem_r):
+        return pltpu.make_async_remote_copy(
+            src_ref=src,
+            dst_ref=dst,
+            send_sem=sem_s,
+            recv_sem=sem_r,
+            device_id=device,
+            device_id_type=MESH,
+        )
+
+    def columns_of(i):
+        return pl.ds(pl.multiple_of(groups[i] * group, 128), group)
+
+    def down(i):
+        dst = targets(groups[i] * nr + r)[2]
+        m = sender[i]
+        remote(dst, dst, zpeer(1), wz_s.at[2, m], wz_r.at[2, m]).wait_recv()
+        for j in range(1, nr):
+            down_r[i, j] = send(dst, dst, peer("r", j), wy_s.at[2, m, j - 1], wy_r.at[2, m, j - 1])
+
+    fed = set()
+
+    def feed(i, f):
+        if i not in fed:
+            fed.add(i)
+            if i == 0:
+                mine[2].wait()
+            for j in range(1, nr):
+                (down_r[i, j] if i else over_r[2, 0, j]).wait_recv()
+        rows = hidden[pl.ds(bases[f], deep)].reshape(deep * tp * share, part)
+
+        def keep(piece, columns):
+            piece = piece.astype(bf).reshape(deep, nc, nx, share, -1)
+            for k in range(nc):
+                part_ref[i, f, k, :, :, :, columns] = piece[:, k]
+
+        if len(downs_ref.shape) == 3:
+            for k in range(nr):
+                piece = jnp.dot(rows, downs_ref[groups[i] * nr + k], preferred_element_type=f32)
+                keep(piece, slice(k * narrow, (k + 1) * narrow))
+        else:
+            keep(jnp.dot(rows, downs_ref[:, columns_of(i)], preferred_element_type=f32), slice(None))
         for l in range(1, nc):
-            hc[k, l].wait_recv()
-        rows = hn_ref[origin[k]].reshape(tp * share, -1)
-        both = jnp.dot(rows, both_ref[...], preferred_element_type=f32)
-        value = jnp.where(fresh, jax.nn.silu(both[:, :part]) * both[:, part:], 0.0)
-        hidden[origin[k]] = value.astype(bf)
-
-    for k in order:
-        with jax.named_scope(f"inner{k}"):
-            inner(k)
-    order = (0,) + far
-    pump(PUMPS[3])
-
-    over_c, over_x, back = {}, {}, {}
-    group = nr * narrow
-
-    def feed(m):
-        if m == 0:
-            mine[2].wait()
-        for j in range(1, nr):
-            over_r[2, m, j].wait_recv()
-        rows = hidden[...].reshape(nz * tp * share, part)
-
-        def keep(piece, columns):
-            piece = piece.astype(bf).reshape(nz, nc, nx, share, -1)
-            for i in range(nc):
-                part_ref[m, i, :, :, :, columns] = piece[:, i]
-
-        if len(downs_ref.shape) == 3:
-            for i in range(nr):
-                piece = jnp.dot(rows, downs_ref[zof(m) * nr + i], preferred_element_type=f32)
-                keep(piece, slice(i * narrow, (i + 1) * narrow))
+            over_c[i, f, l] = send(
+                part_ref.at[i, f, lax.rem(c + l, nc)],
+                got_c.at[i, f, l - 1],
+                peer("c", l),
+                fc_s.at[i, f, l - 1],
+                fc_r.at[i, f, l - 1],
+            )
+
+    def fold_c(i, f):
+        for l in range(1, nc):
+            over_c[i, f, l].wait_recv()
+        for k in range(1, nx + 1):
+            to = lax.rem(x + k, nx)
+            total = part_ref[i, f, c, :, to].astype(f32)
+            for l in range(1, nc):
+                total += got_c[i, f, l - 1, :, to].astype(f32)
+            sum_c[i, f, to] = total.astype(bf)
+            if k < nx:
+                over_x[i, f, k] = send(
+                    sum_c.at[i, f, to],
+                    got_x.at[i, f, k - 1],
+                    peer("x", k),
+                    fx_s.at[i, f, k - 1],
+                    fx_r.at[i, f, k - 1],
+                )
+
+    def fold_x(i, f):
+        for k in range(1, nx):
+            over_x[i, f, k].wait_recv()
+
+        def total(q):
+            value = sum_c[i, f, x, q].astype(f32)
+            for k in range(1, nx):
+                value += got_x[i, f, k - 1, q].astype(f32)
+            return value
+
+        def ship(m, q):
+            at, to = (table[i] for table in landing[m])
+            k = at + inside_i * (to - at)
+            sum_z[i, m - 1] = total(q).astype(bf)
+            back[i, m] = send(
+                sum_z.at[i, m - 1],
+                got_z.at[k, m - 1],
+                zpeer(m),
+                fz_s.at[i, m - 1],
+                fz_r.at[k, m - 1],
+            )
+
+        if f == 0:
+            if nz > 1:
+                ship(1, 1 - lax.rem(z, 2))
+            mid_ref[:, columns_of(i)] += total(lax.rem(z, deep))
         else:
-            columns = pl.ds(pl.multiple_of(zof(m) * group, 128), group)
-            keep(jnp.dot(rows, downs_ref[:, columns], preferred_element_type=f32), slice(None))
-        for l in range(1, nc):
-            over_c[m, l] = send(
-                part_ref.at[m, lax.rem(c + l, nc)],
-                got_c.at[m, l - 1],
-                peer("c", l),
-                fc_s.at[m, l],
-                fc_r.at[m, l],
-            )
-
-    def fold_c(m):
-        for l in range(1, nc):
-            over_c[m, l].wait_recv()
-        for k in range(1, nx + 1):
-            i = lax.rem(x + k, nx)
-            total = part_ref[m, c, :, i].astype(f32)
-            for l in range(1, nc):
-                total += got_c[m, l - 1, :, i].astype(f32)
-            sum_c[m, i] = total.astype(bf)
-            if k < nx:
-                over_x[m, k] = send(
-                    sum_c.at[m, i], got_x.at[m, k - 1], peer("x", k), fx_s.at[m, k], fx_r.at[m, k]
-                )
-
-    def columns_of(m):
-        return pl.ds(pl.multiple_of(zof(m) * group, 128), group)
-
-    def fold_x(m):
-        for k in range(1, nx):
-            over_x[m, k].wait_recv()
-        for p in far + (0,):
-            total = sum_c[m, x, zof(p)].astype(f32)
-            for k in range(1, nx):
-                total += got_x[m, k - 1, zof(p)].astype(f32)
-            if p == 0:
-                mid_ref[:, columns_of(m)] += total
-                continue
-            sum_x[m, p] = total.astype(bf)
-            there = m ^ p
-            back[there, p] = send(
-                sum_x.at[m, p], got_z.at[there, p], zpeer(p), fz_s.at[m, p], fz_r.at[there, p]
-            )
-
-    def close(m):
-        total = mid_ref[:, columns_of(m)]
-        for p in far:
-            back[m, p].wait_recv()
-            total += got_z[m, p].astype(f32)
-        o_ref[:, columns_of(m)] = total.astype(bf)
-
-    plain = ((feed, 0), (pump, 1), (fold_c, 0), (pump, 1), (feed, 1), (fold_c, 1), (pump, 1))
-    plain += ((fold_x, 0), (feed, 2), (fold_c, 2), (fold_x, 1), (feed, 3), (fold_c, 3))
+            for m in (2, 3):
+                ship(m, plan.partner(here, m)["z"] - bases[1])
+
+    def close(i):
+        total = mid_ref[:, columns_of(i)]
+        if nz > 1:
+            for m in far:
+                q = got_z.at[i, m - 1]
+                remote(q, q, zpeer(m), fz_s.at[i, m - 1], fz_r.at[i, m - 1]).wait_recv()
+                total += got_z[i, m - 1].astype(f32)
+        done[:, columns_of(i)] = total.astype(bf)
+        away.append(pltpu.make_async_copy(done.at[:, columns_of(i)], o_ref.at[:, columns_of(i)], local.at[11 + i]))
+        away[-1].start()
+
     def settle(i):
         for copy in over_z.values():
             copy.wait_send()
@@ -633,23 +775,67 @@
             def _():
                 copy.wait_send()
 
-        last = {id(copy) for copy in back.values()}
-        held = streams + [copy for copy in waits if id(copy) not in last]
-        waits[:] = [copy for copy in waits if id(copy) in last]
-        for copy in held:
+        for copy in streams:
             copy.wait_send()
-
-    plain += ((fold_x, 2), (settle, 0), (fold_x, 3), (close, 0), (close, 1), (close, 2), (close, 3))
-    for stage, i in plain:
-        with jax.named_scope(f"{stage.__name__}{i}"):
-            if stage is pump:
-                pump(i)
-            elif i < len(order):
-                stage(order[i])
+        early_ids = {id(copy) for copy in settled}
+        waits[:] = [copy for copy in waits if id(copy) not in early_ids]
+        for copy in settled:
+            copy.wait_send()
+
+    def step(stage, *key):
+        if key[0] < nz and (len(key) < 2 or key[1] < halves):
+            with jax.named_scope(stage.__name__ + "_".join(map(str, key))):
+                stage(*key)
+
+    with jax.named_scope("gateup"):
+        ready()
+    step(inner, 0)
+    step(inner, 1)
+    step(feed, 0, 0)
+    if nz > 1:
+        with jax.named_scope("hnc2"):
+            hn_c(2)
+    step(fold_c, 0, 0)
+    if nz > 1:
+        with jax.named_scope("hnc3"):
+            hn_c(3)
+    step(inner, 2)
+    step(down, 1)
+    step(inner, 3)
+    step(feed, 0, 1)
+    step(fold_c, 0, 1)
+    settled = list(waits)
+    step(fold_x, 0, 0)
+    step(down, 2)
+    step(feed, 1, 0)
+    step(feed, 1, 1)
+    step(fold_c, 1, 0)
+    step(fold_c, 1, 1)
+    step(fold_x, 0, 1)
+    step(down, 3)
+    step(feed, 2, 0)
+    step(feed, 2, 1)
+    step(fold_c, 2, 0)
+    step(fold_c, 2, 1)
+    step(fold_x, 1, 0)
+    step(fold_x, 1, 1)
+    step(settle, 0)
+    step(feed, 3, 1)
+    step(feed, 3, 0)
+    step(fold_c, 3, 1)
+    step(fold_c, 3, 0)
+    step(fold_x, 2, 0)
+    step(fold_x, 2, 1)
+    step(fold_x, 3, 1)
+    step(fold_x, 3, 0)
+    for i in range(4):
+        step(close, i)
     drain()
-
-
-PUMPS = (1, 2, 3, 0)
+    for copy in away:
+        copy.wait()
+
+
+PUMPS = (1, 2)
 
 
 def front(plan, heads, part, args):
@@ -659,7 +845,6 @@
     tok, width = resid.shape
     share = tok // tp
     dma = pltpu.SemaphoreType.DMA
-    vmem = pl.BlockSpec(memory_space=pltpu.VMEM)
     hbm = pl.BlockSpec(memory_space=pl.ANY)
     bf = jnp.bfloat16
     narrow = down.shape[1]
@@ -668,16 +853,18 @@
     proj = (2, plan.sp * tok, heads * NOPE)
     proj = pltpu.VMEM(proj if 4 * proj[1] * proj[2] < 2**23 + 1 else (8, 128), bf)
     more_c, more_x = max(nc - 1, 1), max(nx - 1, 1)
-    sizes = [(nz,), (nz, nr), (nz, nr, nx), (nz, nr, nc), (3, nz), (3, nz, nr), (nc,), (nx,)]
+    more_r = max(nr - 1, 1)
+    sizes = [(nz,), (nz, more_r), (nz, nr, more_x), (nz, nr, more_c), (3, nz), (3, nz, more_r)]
+    sizes += [(more_c,), (more_x,), (5,), (nz, more_x), (nz, more_c)]
+    sizes += [(nz, 2, more_c), (nz, 2, more_x), (nz, 3)]
     sems = [dma(size) for size in sizes for _ in range(2)]
-    sems += [dma((2 * nz, 4)), dma((4,))]
-    sizes = [(nz, nx), (nz, nc), (nz, nc), (nz, nx), (nz, nz)]
-    sems += [dma(size) for size in sizes for _ in range(2)]
+    halves = 2 if nz > 1 else 1
+    deep = nz // halves
     return pl.pallas_call(
         functools.partial(front_body, plan, heads, part),
         out_shape=jax.ShapeDtypeStruct((share, width), bf),
-        in_specs=[vmem] * 8 + [hbm] * 9,
-        out_specs=vmem,
+        in_specs=[hbm] * 17,
+        out_specs=hbm,
         scratch_shapes=[
             pltpu.VMEM((share, width), jnp.float32),
             pltpu.VMEM((nz, nc, nx, share, width), bf),
@@ -685,6 +872,7 @@
             pltpu.VMEM(downs, bf),
             pltpu.VMEM((plan.sp, nc, nx, share, kvl.shape[1] + 2 * ROPE), bf),
             pltpu.VMEM((tok, heads * VDIM), bf),
+            *[pltpu.VMEM(small.shape, small.dtype) for small in args[:8]],
             pltpu.VMEM(wqp.shape, bf),
             pltpu.VMEM(wqr.shape, bf),
             pltpu.VMEM(wk.shape, bf),
@@ -698,14 +886,14 @@
             pltpu.VMEM((more_x, share, width), bf),
             pltpu.VMEM((more_x, share, width), bf),
             pltpu.VMEM((nz, tp * share, part), bf),
-            pltpu.VMEM((nz, nc, nz, nx, share, group), bf),
-            pltpu.VMEM((nz, more_c, nz, nx, share, group), bf),
-            pltpu.VMEM((nz, nx, nz, share, group), bf),
-            pltpu.VMEM((nz, more_x, nz, share, group), bf),
-            pltpu.VMEM((nz, nz, share, group), bf),
-            pltpu.VMEM((nz, nz, share, group), bf),
+            pltpu.VMEM((nz, halves, nc, deep, nx, share, group), bf),
+            pltpu.VMEM((nz, halves, more_c, deep, nx, share, group), bf),
+            pltpu.VMEM((nz, halves, nx, deep, share, group), bf),
+            pltpu.VMEM((nz, halves, more_x, deep, share, group), bf),
+            *[pltpu.VMEM((nz, 3, share, group), bf)] * 2,
+            pltpu.VMEM((share, width), bf),
             *sems,
-            dma((11,)),
+            dma((19 + nz,)),
         ],
         compiler_params=pltpu.CompilerParams(
             collective_id=1, has_side_effects=True, vmem_limit_bytes=62 * 1024 * 1024

time: 121 us -> 112 us (0.926)
  Pallas kernels: 118 us -> 109 us
    pallas_call x1, Pallas kernels: 118 us -> 109 us  [front(): pl.pallas_call(functools.partial(front_body, plan, heads, part), out_shap...]
where the time goes in v2:
time: 112 us
  Pallas kernels  109 us (97%)
  local copies, waits for them, and re-layouts  1.67 us (1%)
  other arithmetic  1.26 us (1%)
    pallas_call x1, Pallas kernels, front(): pl.pallas_call(functools.partial(front_body, plan, heads, part), out_shap...  109 us

profile of v2, /device:TPU:0, one launch (start us, length us, event | category | flops | bytes accessed | tf_op | source)
XLA Modules:
  0.0 111.9 jit_solution(14041671304245211282)
XLA Ops:
  0.0 1.2 %fusion = (f32[256,128]{1,0:T(8,128)}, f32[256,128]{1,0:T(8,128)}) fusion(f32[128]{0:T(128)S(1)} %get-tuple-element.7, f32[128]{0:T(128)S(1)} %get-tuple-element.8, f32[256]{0:T(256)S(1)} %add_convert_fusion), kind=kLoop, calls=%fused_computation.2 | loop fusion | flops 65536 | bytes 264192 | tf_op jit(solution)/shard_map/mul | solution.py:945
  1.3 108.9 %shard_map.145 = bf16[64,2048]{1,0:T(8,128)(2,1)} custom-call(bf16[256,768]{1,0:T(8,128)(2,1)} %ql_hbm.1, bf16[256,512]{1,0:T(8,128)(2,1)} %kvl_hbm.1, bf16[64,256]{1,0:T(8,128)(2,1)} %bitcast.1, f32[768]{0:T(1024)} %qg_hbm.1, f32[512]{0:T(512)} %kg_hbm.1, f32[256,128]{1,0:T(8,128)} %get-tuple-element.6.cos_hbm, f32[256,128]{1,0:T(8,128)} %get-tuple-element.5.sin_hbm, ...), custom_call_target="tpu_custom_call" | custom-call | tf_op jit(solution)/shard_map/pallas_call | solution.py:863
  110.2 1.7 %copy.17 = bf16[64,2048]{1,0:T(8,128)(2,1)} copy(bf16[64,2048]{1,0:T(8,128)(2,1)} %shard_map.145) | data formatting | bytes 524288
  (2 shorter events, 0.0 us)

commit v3 on v2

--- a/solution.py
+++ b/solution.py
@@ -595,6 +595,28 @@
                 for j in range(1, nr):
                     over_r[w, m, j].wait_recv()
 
+    inside_i = jnp.minimum(lax.rem(z, 3), 1)
+    groups = origin
+    sender = (0,) + ((1, 2 + inside_i, 3 - inside_i) if nz > 1 else ())
+    down_r = {}
+
+    def remote(src, dst, device, sem_s, sem_r):
+        return pltpu.make_async_remote_copy(
+            src_ref=src,
+            dst_ref=dst,
+            send_sem=sem_s,
+            recv_sem=sem_r,
+            device_id=device,
+            device_id_type=MESH,
+        )
+
+    def down(i):
+        dst = targets(groups[i] * nr + r)[2]
+        m = sender[i]
+        remote(dst, dst, zpeer(1), wz_s.at[2, m], wz_r.at[2, m]).wait_recv()
+        for j in range(1, nr):
+            down_r[i, j] = send(dst, dst, peer("r", j), wy_s.at[2, m, j - 1], wy_r.at[2, m, j - 1])
+
     for m in far:
         arrange(1, m)
 
@@ -609,6 +631,7 @@
         direct.start()
         waits.append(direct)
         hn_send(hn_z(0, zpeer(3), 2))
+        spread_if(inside, 1, 3)
     hn_x(0)
     if nz > 1:
         with jax.named_scope("upsout"):
@@ -622,7 +645,6 @@
             hn_x(1)
         spread_if(outside, 1, 2)
         spread_if(outside, 2, 1)
-        spread_if(inside, 1, 3)
         with jax.named_scope("hnc0"):
             hn_c(0)
         with jax.named_scope("hn2"):
@@ -630,51 +652,31 @@
             hn_send(hn_z(2, zpeer(1), 2))
             hn_x(2)
         with jax.named_scope("upsin2"):
-            ups(inside, 2)
+            ups(inside, 3, 2)
         with jax.named_scope("hnc1"):
             hn_c(1)
+        spread_if(inside, 2, 1)
+        with jax.named_scope("down1"):
+            down(1)
         with jax.named_scope("hn3"):
             hn_z(3, zpeer(1), 3).wait_recv()
             hn_send(hn_z(3, zpeer(1), 3))
             hn_x(3)
         spread_if(outside, 2, 2, 3)
         spread_if(inside, 2, 3)
-        with jax.named_scope("upsin3"):
-            ups(inside, 3)
-        spread_if(inside, 2, 1, 2)
     else:
         hn_c(0)
 
     group = nr * narrow
     halves = 2 if nz > 1 else 1
     deep = nz // halves
-    inside_i = jnp.minimum(lax.rem(z, 3), 1)
-    groups = origin
-    sender = (0,) + ((1, 2 + inside_i, 3 - inside_i) if nz > 1 else ())
     bases = (2 * half, 2 - 2 * half)[:halves] if nz > 1 else (0,)
     landing = {1: ((1, 0, 2, 3),) * 2, 2: ((3, 2, 0, 1), (2, 3, 1, 0)), 3: ((3, 2, 1, 0), (2, 3, 0, 1))}
     away = []
-    over_c, over_x, down_r, back = {}, {}, {}, {}
-
-    def remote(src, dst, device, sem_s, sem_r):
-        return pltpu.make_async_remote_copy(
-            src_ref=src,
-            dst_ref=dst,
-            send_sem=sem_s,
-            recv_sem=sem_r,
-            device_id=device,
-            device_id_type=MESH,
-        )
+    over_c, over_x, back = {}, {}, {}
 
     def columns_of(i):
         return pl.ds(pl.multiple_of(groups[i] * group, 128), group)
-
-    def down(i):
-        dst = targets(groups[i] * nr + r)[2]
-        m = sender[i]
-        remote(dst, dst, zpeer(1), wz_s.at[2, m], wz_r.at[2, m]).wait_recv()
-        for j in range(1, nr):
-            down_r[i, j] = send(dst, dst, peer("r", j), wy_s.at[2, m, j - 1], wy_r.at[2, m, j - 1])
 
     fed = set()
 
@@ -787,45 +789,52 @@
             with jax.named_scope(stage.__name__ + "_".join(map(str, key))):
                 stage(*key)
 
+    def last(when):
+        if nz > 1:
+
+            @pl.when(when)
+            def _():
+                with jax.named_scope("hnc3"):
+                    hn_c(3)
+
+    if nz > 1:
+        with jax.named_scope("hnc2"):
+            hn_c(2)
+    last(inside)
     with jax.named_scope("gateup"):
         ready()
+    spread_if(inside, 2, 2)
     step(inner, 0)
     step(inner, 1)
     step(feed, 0, 0)
-    if nz > 1:
-        with jax.named_scope("hnc2"):
-            hn_c(2)
+    step(inner, 2)
     step(fold_c, 0, 0)
-    if nz > 1:
-        with jax.named_scope("hnc3"):
-            hn_c(3)
-    step(inner, 2)
-    step(down, 1)
+    step(feed, 1, 0)
+    last(outside)
+    step(fold_c, 1, 0)
     step(inner, 3)
     step(feed, 0, 1)
+    step(feed, 1, 1)
     step(fold_c, 0, 1)
-    settled = list(waits)
+    step(fold_c, 1, 1)
     step(fold_x, 0, 0)
     step(down, 2)
-    step(feed, 1, 0)
-    step(feed, 1, 1)
-    step(fold_c, 1, 0)
-    step(fold_c, 1, 1)
+    step(fold_x, 1, 0)
     step(fold_x, 0, 1)
+    settled = list(waits)
     step(down, 3)
+    step(fold_x, 1, 1)
+    step(feed, 2, 1)
     step(feed, 2, 0)
-    step(feed, 2, 1)
+    step(fold_c, 2, 1)
     step(fold_c, 2, 0)
-    step(fold_c, 2, 1)
-    step(fold_x, 1, 0)
-    step(fold_x, 1, 1)
-    step(settle, 0)
     step(feed, 3, 1)
     step(feed, 3, 0)
     step(fold_c, 3, 1)
     step(fold_c, 3, 0)
+    step(settle, 0)
+    step(fold_x, 2, 1)
     step(fold_x, 2, 0)
-    step(fold_x, 2, 1)
     step(fold_x, 3, 1)
     step(fold_x, 3, 0)
     for i in range(4):

time: 112 us -> 112 us (level)
  no operation moved by 1% of the time
where the time goes in v3:
time: 112 us
  Pallas kernels  109 us (97%)
  local copies, waits for them, and re-layouts  1.67 us (1%)
  other arithmetic  1.26 us (1%)
    pallas_call x1, Pallas kernels, front(): pl.pallas_call(functools.partial(front_body, plan, heads, part), out_shap...  109 us

profile of v3, /device:TPU:0, one launch (start us, length us, event | category | flops | bytes accessed | tf_op | source)
XLA Modules:
  0.0 111.7 jit_solution(223794106961332508)
XLA Ops:
  0.0 1.2 %fusion = (f32[256,128]{1,0:T(8,128)}, f32[256,128]{1,0:T(8,128)}) fusion(f32[128]{0:T(128)S(1)} %get-tuple-element.7, f32[128]{0:T(128)S(1)} %get-tuple-element.8, f32[256]{0:T(256)S(1)} %add_convert_fusion), kind=kLoop, calls=%fused_computation.2 | loop fusion | flops 65536 | bytes 264192 | tf_op jit(solution)/shard_map/mul | solution.py:954
  1.3 108.8 %shard_map.145 = bf16[64,2048]{1,0:T(8,128)(2,1)} custom-call(bf16[256,768]{1,0:T(8,128)(2,1)} %ql_hbm.1, bf16[256,512]{1,0:T(8,128)(2,1)} %kvl_hbm.1, bf16[64,256]{1,0:T(8,128)(2,1)} %bitcast.1, f32[768]{0:T(1024)} %qg_hbm.1, f32[512]{0:T(512)} %kg_hbm.1, f32[256,128]{1,0:T(8,128)} %get-tuple-element.6.cos_hbm, f32[256,128]{1,0:T(8,128)} %get-tuple-element.5.sin_hbm, ...), custom_call_target="tpu_custom_call" | custom-call | tf_op jit(solution)/shard_map/pallas_call | solution.py:872
  110.1 1.7 %copy.17 = bf16[64,2048]{1,0:T(8,128)(2,1)} copy(bf16[64,2048]{1,0:T(8,128)(2,1)} %shard_map.145) | data formatting | bytes 524288
  (2 shorter events, 0.0 us)
